TPU v7x, 32 devices: a whole 2x2x4 slice. The times are simulated.
32 devices in a mesh: sp: 8 (over z, x), tp: 4 (over y, core).
Axes of the slice: x: 2, y: 2, z: 4, core: 2. Of those that a mesh axis runs over, the one named last changes fastest.
Arguments:
- inputs: bfloat16 [3072, 2048], P('sp', 'tp'), may hold values from -6 to 6
- norm_gain: float32 [2048], replicated, may hold values from 0.1 to 1.9
- query_weight: bfloat16 [2048, 1024], P(None, 'tp')
- key_weight: bfloat16 [2048, 1024], P(None, 'tp'), may hold values from -0.15625 to 0.15625
- value_weight: bfloat16 [2048, 1024], P(None, 'tp'), may hold values from -0.125 to 0.125
- memory_query_weight: bfloat16 [2048, 1024], P(None, 'tp'), may hold values from -0.125 to 0.125
- memory_key_weight: bfloat16 [2048, 1024], P(None, 'tp'), may hold values from -0.125 to 0.125
- memory_value_weight: bfloat16 [2048, 1024], P(None, 'tp'), may hold values from -0.125 to 0.125
- input_gate_weight: bfloat16 [2048, 16], P(None, 'tp')
- forget_gate_weight: bfloat16 [2048, 16], P(None, 'tp'), may hold values from -0.3125 to 0.3125
- forget_bias: float32 [16], P('tp'), may hold values from 3 to 13
- decay_shift: float32 [3072, 16], P('sp', 'tp'), may hold values from -2 to 0, as said below
- lambdas: float32 [16], P('tp'), may hold values from 0.3 to 0.8
- head_gain: float32 [64], replicated, may hold values from 0.1 to 1.9
- out_weight_attention: bfloat16 [1024, 2048], P('tp'), may hold values from -0.125 to 0.125
- out_weight_memory: bfloat16 [1024, 2048], P('tp'), may hold values from -0.125 to 0.125
Outputs:
- combined: bfloat16 [3072, 2048], P('sp', 'tp')
Inputs may be any that keep to these rules, and one draw needn't show every extreme that they name: `decay_shift`: never positive.
All inputs are finite; a program needn't handle non-finite values.
Results may differ from a plain program's by a relative error of at most 0.018.
The roundings to bfloat16 on the way count: a program that leaves them out, or rounds other values in their place, can miss the bound.
Values may be sent and summed in bfloat16 or wider, within the bound.
A program may use at most 192 MiB of HBM per device.

v0:
```python
import jax
import jax.numpy as jnp
from jax import lax
from jax.sharding import PartitionSpec as P

HEAD = 64
DD = 32
BLOCK = 64
EPSILON = 1e-06
ROTARY_BASE = 10000.0
NEGATIVE = -1e30


def carried_in(part, axis, combine, identity):
    place = lax.axis_index(axis)
    gathered = jax.tree.map(lambda a: lax.all_gather(a, axis), part)
    state = jax.tree.map(lambda a, e: jnp.zeros_like(a) + jnp.asarray(e, a.dtype), part, identity)

    def one(hop, state):
        return combine(
            state, jax.tree.map(lambda a: lax.dynamic_index_in_dim(a, hop, 0, False), gathered)
        )

    return lax.fori_loop(0, place, one, state)


def rotate(halves, positions):
    middle = halves.shape[-1] // 2
    inverse = 1.0 / ROTARY_BASE ** (jnp.arange(middle, dtype=jnp.float32) / middle)
    angles = positions.astype(jnp.float32)[:, None] * inverse[None, :]
    cosine = jnp.cos(angles)[:, None, :]
    sine_part = jnp.sin(angles)[:, None, :]
    floats = halves.astype(jnp.float32)
    former = floats[..., :middle]
    latter = floats[..., middle:]
    turned = jnp.concatenate(
        [former * cosine - latter * sine_part, latter * cosine + former * sine_part], axis=-1
    )
    return turned.astype(jnp.bfloat16)


def advance_state(carried, block_entry):
    memory, normal, stable = carried
    block_memory, block_normal, block_max, block_decay = block_entry
    new_stable = jnp.maximum(block_decay + stable, block_max)
    former = jnp.exp(block_decay + stable - new_stable)
    latter = jnp.exp(block_max - new_stable)
    return (
        former[:, None, None] * memory + latter[:, None, None] * block_memory,
        former[:, None] * normal + latter[:, None] * block_normal,
        new_stable,
    )


def memory_blocks(queries, key_heads, values, gate_in, log_forget, entering):
    token_count, head_count, head_width = queries.shape
    block_count = token_count // BLOCK
    highest = lax.Precision.HIGHEST

    def blocked(flat_array):
        return (
            flat_array.astype(jnp.float32)
            .reshape(block_count, BLOCK, head_count, head_width)
            .transpose(2, 0, 1, 3)
        )

    query_blocks = blocked(queries)
    key_blocks = blocked(key_heads) * head_width ** (-0.5)
    value_blocks = blocked(values)
    gate_blocks = gate_in.reshape(block_count, BLOCK, head_count).transpose(2, 0, 1)
    cumulative = jnp.cumsum(
        log_forget.reshape(block_count, BLOCK, head_count).transpose(2, 0, 1), axis=-1
    )
    block_ends = cumulative[..., -1]
    toward_end = block_ends[..., None] - cumulative + gate_blocks
    local_max = jnp.max(toward_end, axis=-1)
    end_weights = jnp.exp(toward_end - local_max[..., None])
    local_memory = jnp.einsum(
        "hcl,hclv,hclk->chvk", end_weights, value_blocks, key_blocks, precision=highest
    )
    local_normal = jnp.einsum("hcl,hclk->chk", end_weights, key_blocks, precision=highest)

    def scan_step(carried, block_entry):
        return (advance_state(carried, block_entry), carried)

    entries = (local_memory, local_normal, local_max.T, block_ends.T)
    unused, (memory_in, normal_in, stable_in) = lax.scan(scan_step, entering, entries)
    lower_mask = jnp.tril(jnp.ones((BLOCK, BLOCK), dtype=bool))
    decays = jnp.where(
        lower_mask,
        cumulative[..., :, None] - cumulative[..., None, :] + gate_blocks[..., None, :],
        NEGATIVE,
    )
    carried_log = cumulative + stable_in.T[..., None]
    row_max = jnp.maximum(carried_log, jnp.max(decays, axis=-1))
    within = jnp.where(lower_mask, jnp.exp(decays - row_max[..., None]), 0.0)
    outside = jnp.exp(carried_log - row_max)
    scores = within * jnp.einsum("hctd,hcsd->hcts", query_blocks, key_blocks, precision=highest)
    numerator = outside[..., None] * jnp.einsum(
        "chvk,hctk->hctv", memory_in, query_blocks, precision=highest
    )
    numerator = numerator + jnp.einsum("hcts,hcsv->hctv", scores, value_blocks, precision=highest)
    denominator = outside * jnp.einsum(
        "chk,hctk->hct", normal_in, query_blocks, precision=highest
    ) + jnp.sum(scores, axis=-1)
    result = numerator / jnp.maximum(jnp.abs(denominator), 1.0)[..., None]
    return (
        result.transpose(1, 2, 0, 3)
        .reshape(token_count, head_count * head_width)
        .astype(jnp.bfloat16)
    )


def combine_states(earlier, later_part):
    memory, normal, stable, decay_sum = earlier
    later_memory, later_normal, later_stable, later_decay = later_part
    new_stable = jnp.maximum(later_decay + stable, later_stable)
    former = jnp.exp(later_decay + stable - new_stable)
    latter = jnp.exp(later_stable - new_stable)
    return (
        former[:, None, None] * memory + latter[:, None, None] * later_memory,
        former[:, None] * normal + latter[:, None] * later_normal,
        new_stable,
        decay_sum + later_decay,
    )


def summarize(key_heads, values, gate_in, log_forget):
    head_width = key_heads.shape[-1]
    highest = lax.Precision.HIGHEST
    key_floats = key_heads.astype(jnp.float32) * head_width ** (-0.5)
    cumulative = jnp.cumsum(log_forget, axis=0)
    span_decay = cumulative[-1]
    toward_end = span_decay[None, :] - cumulative + gate_in
    span_max = jnp.max(toward_end, axis=0)
    end_weights = jnp.exp(toward_end - span_max[None, :])
    memory = jnp.einsum(
        "rh,rhv,rhk->hvk", end_weights, values.astype(jnp.float32), key_floats, precision=highest
    )
    normal = jnp.einsum("rh,rhk->hk", end_weights, key_floats, precision=highest)
    return (memory, normal, span_max, span_decay)


def attend(carried, arriving, query_first, query_second, query_positions):
    key_first = arriving[..., :DD]
    key_second = arriving[..., DD : 2 * DD]
    value_part = arriving[..., 2 * DD :]
    key_positions = jnp.arange(arriving.shape[0], dtype=jnp.int32)
    visible = (key_positions[None, :] <= query_positions[:, None]) & (key_positions[None, :] >= 0)
    score_scale = DD ** (-0.5)
    results = []
    for side_index, (query_side, key_side) in enumerate(
        ((query_first, key_first), (query_second, key_second))
    ):
        row_max, totals, accumulated = carried[3 * side_index : 3 * side_index + 3]
        scores = (
            jnp.einsum("qhd,khd->hqk", query_side, key_side, preferred_element_type=jnp.float32)
            * score_scale
        )
        scores = jnp.where(visible[None], scores, NEGATIVE)
        new_max = jnp.maximum(row_max, jnp.max(scores, axis=2))
        weights = jnp.where(visible[None], jnp.exp(scores - new_max[..., None]), 0.0)
        totals = jnp.sum(weights, axis=2)
        accumulated = jnp.einsum(
            "hqk,khd->hqd",
            weights.astype(jnp.bfloat16),
            value_part,
            preferred_element_type=jnp.float32,
        )
        results.extend([new_max, totals, accumulated])
    return tuple(results)


def per_device(
    inputs,
    norm_gain,
    query_weight,
    key_weight,
    value_weight,
    memory_query_weight,
    memory_key_weight,
    memory_value_weight,
    input_gate_weight,
    forget_gate_weight,
    forget_bias,
    decay_shift,
    lambdas,
    head_gain,
    out_weight_attention,
    out_weight_memory,
):
    row_count = inputs.shape[0]
    weights = (
        query_weight,
        key_weight,
        value_weight,
        memory_query_weight,
        memory_key_weight,
        memory_value_weight,
        input_gate_weight,
        forget_gate_weight,
    )
    floats = lax.all_gather(inputs, "tp", axis=1, tiled=True).astype(jnp.float32)
    scaled = (floats * norm_gain[None, :]).astype(jnp.bfloat16)
    running_sums = tuple(
        (jnp.dot(scaled, weight, preferred_element_type=jnp.float32) for weight in weights)
    )
    running_sums, squares = (running_sums, jnp.sum(floats * floats, axis=1))
    inverse_rms = lax.rsqrt(squares / norm_gain.shape[0] + EPSILON)[:, None]
    projected = [running * inverse_rms for running in running_sums]

    def split_heads(flat_values):
        return flat_values.astype(jnp.bfloat16).reshape(row_count, -1, HEAD)

    queries = split_heads(projected[0])
    key_heads = split_heads(projected[1])
    values = split_heads(projected[2])
    offset = lax.axis_index("sp") * row_count
    positions = offset + jnp.arange(row_count, dtype=jnp.int32)
    query_first = rotate(queries[..., :DD], positions)
    query_second = rotate(queries[..., DD:], positions)
    packed = jnp.concatenate(
        [rotate(key_heads[..., :DD], positions), rotate(key_heads[..., DD:], positions), values],
        axis=-1,
    )
    head_count = queries.shape[1]
    empty_max = jnp.full((head_count, row_count), NEGATIVE, jnp.float32)
    empty_total = jnp.zeros((head_count, row_count), jnp.float32)
    empty_sums = jnp.zeros((head_count, row_count, HEAD), jnp.float32)
    starting = (empty_max, empty_total, empty_sums, empty_max, empty_total, empty_sums)
    gathered = attend(
        starting,
        lax.all_gather(packed, "sp", axis=0, tiled=True),
        query_first,
        query_second,
        positions,
    )
    first_max, first_total, first_sums, second_max, second_total, second_sums = gathered
    stacked = first_sums / first_total[..., None] - lambdas[:, None, None] * (
        second_sums / second_total[..., None]
    )
    stacked = stacked.transpose(1, 0, 2)
    norm_scale = lax.rsqrt(jnp.mean(stacked * stacked, axis=-1, keepdims=True) + EPSILON)
    attended = (stacked * norm_scale * head_gain).astype(jnp.bfloat16).reshape(row_count, -1)
    gate_in = projected[6]
    log_forget = jax.nn.log_sigmoid(projected[7] + forget_bias[None, :]) + decay_shift
    memory_queries = split_heads(projected[3])
    memory_keys = split_heads(projected[4])
    memory_values = split_heads(projected[5])
    summary = summarize(memory_keys, memory_values, gate_in, log_forget)
    memory_heads = gate_in.shape[1]
    identity = (
        jnp.zeros((memory_heads, HEAD, HEAD), jnp.float32),
        jnp.zeros((memory_heads, HEAD), jnp.float32),
        jnp.full((memory_heads,), NEGATIVE, jnp.float32),
        jnp.zeros((memory_heads,), jnp.float32),
    )
    prefix = carried_in(summary, "sp", combine_states, identity)
    start_state = (
        jnp.zeros((memory_heads, HEAD, HEAD), jnp.float32),
        jnp.zeros((memory_heads, HEAD), jnp.float32),
        jnp.zeros((memory_heads,), jnp.float32),
        jnp.zeros((memory_heads,), jnp.float32),
    )
    entering = combine_states(start_state, prefix)[:3]
    memory = memory_blocks(
        memory_queries, memory_keys, memory_values, gate_in, log_forget, entering
    )
    partial_term = jnp.dot(attended, out_weight_attention, preferred_element_type=jnp.float32)
    partial_term = partial_term + jnp.dot(
        memory, out_weight_memory, preferred_element_type=jnp.float32
    )
    return lax.psum_scatter(
        partial_term.astype(jnp.bfloat16), "tp", scatter_dimension=1, tiled=True
    )


def solution(mesh):
    in_specs = (
        P("sp", "tp"),
        P(),
        P(None, "tp"),
        P(None, "tp"),
        P(None, "tp"),
        P(None, "tp"),
        P(None, "tp"),
        P(None, "tp"),
        P(None, "tp"),
        P(None, "tp"),
        P("tp"),
        P("sp", "tp"),
        P("tp"),
        P(),
        P("tp", None),
        P("tp", None),
    )
    out_specs = P("sp", "tp")
    return jax.shard_map(
        per_device, mesh=mesh, in_specs=in_specs, out_specs=out_specs, check_vma=False
    )
```

profile of v0, /device:TPU:0, one launch (start us, length us, event | category | flops | bytes accessed | tf_op | source)
XLA Modules:
  0.0 310.0 jit_solution(3127829194106254127)
XLA Ops:
  10.2 21.1 %all-gather.8.cloned.1.call-done = bf16[384,2048]{1,0:T(8,128)(2,1)} async-done(((bf16[384,512]{1,0:T(8,128)(2,1)}), bf16[384,2048]{1,0:T(8,128)(2,1)}) %all-gather.8.cloned.1.call-update) | async-done | bytes 1572880 | tf_op jit(solution)/shard_map/all_gather | solution.py:203
  31.3 1.8 fusion.26
  33.2 1.9 fusion.113
  37.0 2.0 fusion.128
  39.5 21.3 %all-reduce = f32[32]{0:T(128)S(1)} all-reduce(f32[32]{0:T(128)S(1)} %dynamic-update-slice), channel_id=2, replica_groups=mesh['sp'=8,'tp'=4] {'sp'}, use_global_device_ids=true, to_apply=%add | all-reduce | flops 32 | bytes 256
  60.9 16.7 %all-gather.3 = f32[8,1,4]{2,1,0:T(1,128)} all-gather(f32[1,1,4]{2,1,0:T(1,128)S(1)} %bitcast.225), channel_id=1, replica_groups=mesh['sp'=8,'tp'=4] {'sp'}, dimensions={0}, use_global_device_ids=true | all-gather | bytes 144 | tf_op jit(solution)/shard_map/all_gather | solution.py:16
  79.6 2.5 fusion.46
  83.3 2.5 fusion.49
  88.5 26.1 %all-gather.4 = f32[8,4,64]{2,1,0:T(4,128)S(1)} all-gather(f32[1,4,64]{2,1,0:T(4,128)S(1)} %bitcast.221), channel_id=4, replica_groups=mesh['sp'=8,'tp'=4] {'sp'}, dimensions={0}, use_global_device_ids=true | all-gather | bytes 9216 | tf_op jit(solution)/shard_map/all_gather | solution.py:16
  114.6 2.5 fusion.44
  122.4 2.3 fusion.78
  124.7 36.9 %all-gather.1 = f32[32,64,64]{2,1,0:T(8,128)} all-gather(f32[4,64,64]{2,1,0:T(8,128)S(1)} %copy-done.7), channel_id=3, replica_groups=mesh['sp'=8,'tp'=4] {'sp'}, dimensions={0}, use_global_device_ids=true | all-gather | bytes 589824 | tf_op jit(solution)/shard_map/all_gather | solution.py:16
  162.0 18.5 %while.37 = (s32[]{:T(128)}, f32[4,64,64]{2,1,0:T(8,128)S(1)}, f32[4,64]{1,0:T(4,128)S(1)}, f32[4]{0:T(128)S(1)}, f32[6,4,64,64]{3,2,0,1:T(8,128)}, /*index=5*/f...) while((s32[]{:T(128)}, f32[4,64,64]{2,1,0:T(8,128)S(1)}, ...), condition=%wide.region_14.15_spmd, body=%wide.region_13.14_spmd.sunk | while | flops 49938 | bytes 399745 | solution.py:87
  180.5 3.1 %fusion.50 = bf16[384,256]{0,1:T(8,128)(2,1)} fusion(bf16[2048,256]{1,0:T(8,128)(2,1)} %param.25, bf16[384,2048]{1,0:T(8,128)(2,1)} %all-gather.8.cloned.1.call-done, f32[2048]{0:T(1024)S(1)} %copy-done.22, f32[384]{0:T(512)S(1)} %copy-done.11), kind=kOutput, calls=%fused_computation.71 | convolution fusion | flops 405209088 | bytes 2827776 | tf_op jit(solution)/shard_map/dot_general | solution.py:206
  183.6 1.8 copy.64
  185.4 1.9 reshape.199
  187.3 1.9 copy.80
  195.7 2.5 fusion.43
  198.3 10.2 %fusion.75 = f32[4,384,3072]{2,1,0:T(8,128)} fusion(bf16[3072,4,128]{0,2,1:T(8,128)(2,1)} %all-gather.10.cloned.1.call-done, bf16[384,4,16]{0,2,1:T(8,128)(2,1)S(1)} %get-tuple-element.253, bf16[384,4,16]{0,2,1:T(8,128)(2,1)S(1)} %get-tuple-element.254), kind=kOutput, calls=%fused_computation.82 | convolution fusion | flops 302186496 | bytes 19759104 | tf_op jit(solution)/shard_map/qhd,khd->hqk/dot_general | solution.py:157
  208.5 17.6 %fusion.14 = (f32[4,384]{1,0:T(4,128)S(1)}, f32[4,384]{1,0:T(4,128)S(1)}, f32[4,384,3072]{2,1,0:T(8,128)}) fusion(pred[384,3072]{1,0:T(8,128)(4,1)S(1)} %iota_compare_fusion, f32[4,384,3072]{2,1,0:T(8,128)} %fusion.75, bf16[3072,4,128]{0,2,1:T(8,128)(2,1)} %all-gather.10.cloned.1.call-done, bf16[384,4,16]{0,2,1:T(8,128)(2,1)S(1)} %get-tuple-element.246, ...), kind=kOutput, calls=%fused_computation.32 | convolution fusion | flops 330494976 | bytes 39825408 | tf_op jit(solution)/shard_map/qhd,khd->hqk/dot_general | solution.py:157
  226.1 17.6 %fusion.17 = (f32[4,384]{1,0:T(4,128)S(1)}, f32[4,384]{1,0:T(4,128)S(1)}) fusion(f32[4,384,3072]{2,1,0:T(8,128)} %get-tuple-element.257, f32[4,384]{1,0:T(4,128)S(1)} %get-tuple-element.264, pred[384,3072]{1,0:T(8,128)(4,1)} %copy-done.2, f32[4,384]{1,0:T(4,128)S(1)} %get-tuple-element.265, f32[4,384,3072]{2,1,0:T(8,128)} %fusion.75), kind=kLoop, calls=%fused_computation.35 | loop fusion | flops 47182848 | bytes 38952960 | tf_op jit(solution)/shard_map/reduce_sum | solution.py:163
  244.0 8.0 %fusion.68 = f32[384,4,64]{0,2,1:T(8,128)S(1)} fusion(bf16[3072,4,128]{0,2,1:T(8,128)(2,1)} %all-gather.10.cloned.1.call-done, f32[4,384,3072]{2,1,0:T(8,128)S(1)} %copy-done.1, f32[4,384]{1,0:T(4,128)S(1)} %get-tuple-element.265, pred[384,3072]{1,0:T(8,128)(4,1)} %copy-done.2, f32[384,4]{0,1:T(4,128)S(1)} %bitcast.224), kind=kOutput, calls=%fused_computation.79 | convolution fusion | flops 627671040 | bytes 22032384 | tf_op jit(solution)/shard_map/hqk,khd->hqd/dot_general | solution.py:164
  252.0 9.9 %multiply_reduce_fusion = (f32[384,4]{0,1:T(4,128)S(1)}, f32[384,4,64]{0,2,1:T(8,128)S(1)}) fusion(f32[384,4,64]{0,2,1:T(8,128)S(1)} %fusion.68, f32[384,4]{0,1:T(4,128)S(1)} %bitcast.223, bf16[3072,4,128]{0,2,1:T(8,128)(2,1)} %all-gather.10.cloned.1.call-done, f32[4,384,3072]{2,1,0:T(8,128)} %get-tuple-element.257, f32[4,384]{1,0:T(4,128)S(1)} %get-tuple-element.264, ...), kind=kOutput, calls=%fused_computation.97 | convolution fusion | flops 628062720 | bytes 22431760 | tf_op jit(solution)/shard_map/hqk,khd->hqd/dot_general | solution.py:164
  264.9 38.5 %reduce-scatter.2.cloned.1.call-done = bf16[384,512]{1,0:T(8,128)(2,1)} async-done(((bf16[384,2048]{1,0:T(8,128)(2,1)}), bf16[384,512]{1,0:T(8,128)(2,1)}) %reduce-scatter.2.cloned.1.call-update) | async-done | bytes 393232 | tf_op jit(solution)/shard_map/reduce_scatter | solution.py:273
  (176 shorter events, 44.7 us)
Async XLA Ops:
  6.5 255.5 %copy-start = (bf16[256,2048]{1,0:T(8,128)(2,1)S(1)}, bf16[256,2048]{1,0:T(8,128)(2,1)}, u32[]{:S(2)}) copy-start(bf16[256,2048]{1,0:T(8,128)(2,1)} %param.34) | copy-start | bytes 3145732
  6.5 26.6 %copy-start.19 = (f32[2048]{0:T(1024)S(1)}, f32[2048]{0:T(1024)}, u32[]{:S(2)}) copy-start(f32[2048]{0:T(1024)} %param.21) | copy-start | bytes 24580
  6.5 26.6 %copy-start.24 = (f32[384,4]{0,1:T(4,128)S(1)}, f32[384,4]{0,1:T(4,128)}, u32[]{:S(2)}) copy-start(f32[384,4]{0,1:T(4,128)} %param.31) | copy-start | bytes 18436
  6.5 26.6 %copy-start.25 = (f32[4]{0:T(128)S(1)}, f32[4]{0:T(128)}, u32[]{:S(2)}) copy-start(f32[4]{0:T(128)} %param.30) | copy-start | bytes 52
  6.5 26.6 %copy-start.16 = (bf16[2048,4]{0,1:T(4,128)(2,1)S(1)}, bf16[2048,4]{0,1:T(4,128)(2,1)}, u32[]{:S(2)}) copy-start(bf16[2048,4]{0,1:T(4,128)(2,1)} %param.29) | copy-start | bytes 49156
  6.5 30.5 %copy-start.17 = (bf16[2048,4]{0,1:T(4,128)(2,1)S(1)}, bf16[2048,4]{0,1:T(4,128)(2,1)}, u32[]{:S(2)}) copy-start(bf16[2048,4]{0,1:T(4,128)(2,1)} %param.28) | copy-start | bytes 49156
  6.6 24.8 %all-gather.8.cloned.1.call-start = ((), (), s32[]{:S(2)}) async-start(), calls=%async_computation.1 | async-start | bytes 1966080 | tf_op jit(solution)/shard_map/all_gather | solution.py:203
  7.3 191.0 %all-gather.10.cloned.1.call-start = ((), (), s32[]{:S(2)}) async-start(), calls=%async_computation.2 | async-start | bytes 3538944 | tf_op jit(solution)/shard_map/all_gather | solution.py:233
  10.2 198.3 %copy-start.2 = (pred[384,3072]{1,0:T(8,128)(4,1)}, pred[384,3072]{1,0:T(8,128)(4,1)S(1)}, u32[]{:S(2)}) copy-start(pred[384,3072]{1,0:T(8,128)(4,1)S(1)} %iota_compare_fusion) | copy-start | bytes 3538948
  33.2 84.0 %copy-start.10 = (f32[384]{0:T(512)}, f32[384]{0:T(512)S(1)}, u32[]{:S(2)}) copy-start(f32[384]{0:T(512)S(1)} %add_rsqrt_fusion.1) | copy-start | bytes 4612
  82.5 38.5 %copy-start.3 = (bf16[6,64,4,64]{3,2,1,0:T(4,128)(2,1)}, bf16[6,64,4,64]{3,2,1,0:T(4,128)(2,1)S(1)}, u32[]{:S(2)}) copy-start(bf16[6,64,4,64]{3,2,1,0:T(4,128)(2,1)S(1)} %reshape.198) | copy-start | bytes 589828
  82.5 32.1 %copy-start.20 = (f32[2048]{0:T(1024)S(1)}, f32[2048]{0:T(1024)}, u32[]{:S(2)}) copy-start(f32[2048]{0:T(1024)} %param.21) | copy-start | bytes 24580
  86.7 30.5 %copy-start.5 = (bf16[384,2048]{1,0:T(8,128)(2,1)S(1)}, bf16[384,2048]{1,0:T(8,128)(2,1)}, u32[]{:S(2)}) copy-start(bf16[384,2048]{1,0:T(8,128)(2,1)} %all-gather.8.cloned.1.call-done) | copy-start | bytes 4718596
  86.7 30.5 %copy-start.14 = (bf16[2048,256]{1,0:T(8,128)(2,1)S(1)}, bf16[2048,256]{1,0:T(8,128)(2,1)}, u32[]{:S(2)}) copy-start(bf16[2048,256]{1,0:T(8,128)(2,1)} %param.24) | copy-start | bytes 3145732
  86.7 30.5 %copy-start.21 = (f32[2048]{0:T(1024)S(1)}, f32[2048]{0:T(1024)}, u32[]{:S(2)}) copy-start(f32[2048]{0:T(1024)} %param.21) | copy-start | bytes 24580
  118.8 184.6 %reduce-scatter.2.cloned.1.call-start = ((), (), s32[]{:S(2)}) async-start(), calls=%async_computation.3 | async-start | bytes 1966080 | tf_op jit(solution)/shard_map/reduce_scatter | solution.py:273
  161.6 18.9 %copy-start.11 = (f32[384]{0:T(512)S(1)}, f32[384]{0:T(512)}, u32[]{:S(2)}) copy-start(f32[384]{0:T(512)} %copy-done.10) | copy-start | bytes 4612
  161.6 18.9 %copy-start.22 = (f32[2048]{0:T(1024)S(1)}, f32[2048]{0:T(1024)}, u32[]{:S(2)}) copy-start(f32[2048]{0:T(1024)} %param.21) | copy-start | bytes 24580
  180.5 9.6 %copy-start.18 = (f32[6,4,64]{2,1,0:T(4,128)S(1)}, f32[6,4,64]{2,1,0:T(4,128)}, u32[]{:S(2)}) copy-start(f32[6,4,64]{2,1,0:T(4,128)} %get-tuple-element.126) | copy-start | bytes 18436
  183.6 9.7 %copy-start.4 = (bf16[6,64,4,64]{3,2,1,0:T(4,128)(2,1)S(1)}, bf16[6,64,4,64]{3,2,1,0:T(4,128)(2,1)}, u32[]{:S(2)}) copy-start(bf16[6,64,4,64]{3,2,1,0:T(4,128)(2,1)} %copy-done.3) | copy-start | bytes 589828
  189.5 4.7 %copy-start.15 = (f32[6,4,64,64]{3,2,0,1:T(8,128)S(1)}, f32[6,4,64,64]{3,2,0,1:T(8,128)}, u32[]{:S(2)}) copy-start(f32[6,4,64,64]{3,2,0,1:T(8,128)} %get-tuple-element.125) | copy-start | bytes 1179652
  226.1 17.9 %copy-start.1 = (f32[4,384,3072]{2,1,0:T(8,128)S(1)}, f32[4,384,3072]{2,1,0:T(8,128)}, u32[]{:S(2)}) copy-start(f32[4,384,3072]{2,1,0:T(8,128)} %fusion.75) | copy-start | bytes 56623108
  244.0 8.0 %copy-start.26 = (f32[4]{0:T(128)S(1)}, f32[4]{0:T(128)}, u32[]{:S(2)}) copy-start(f32[4]{0:T(128)} %param.32) | copy-start | bytes 52
  252.0 9.9 %copy-start.13 = (f32[64]{0:T(128)S(1)}, f32[64]{0:T(128)}, u32[]{:S(2)}) copy-start(f32[64]{0:T(128)} %param.33) | copy-start | bytes 772
  (6 other events, 15.8 us)
Sparse Core Ops, SparseCore 0:
  8.9 22.3 all-gather.7
  118.9 66.6 all-gather.9
  265.0 38.3 reduce-scatter.1
where the time goes:
time: 311 us; the launch traced here: 310 us
  blocking collectives  101 us (32%)
  matrix products  75.5 us (24%)
  waiting for transfers between devices  60.4 us (19%)
  other arithmetic  36.2 us (12%)
  local copies, waits for them, and re-layouts  22.1 us (7%)
  between operations  14.4 us (5%)
    all_gather x3, blocking collectives, carried_in(): gathered = jax.tree.map(lambda a: lax.all_gather(a, axis), part)  79.7 us
    reduce_scatter x1, waiting for transfers between devices, per_device(): lax.psum_scatter(partial_term.astype(jnp.bfloat16), 'tp', scatter_dimensi...  38.5 us
    dot_general x2, matrix products, attend(): jnp.einsum('qhd,khd->hqk', query_side, key_side, preferred_element_type=j...  27.8 us
    unnamed x1, blocking collectives  21.3 us
    all_gather x1, waiting for transfers between devices, per_device(): lax.all_gather(inputs, 'tp', axis=1, tiled=True).astype(jnp.float32)  21.1 us
    dot_general x2, matrix products, attend(): jnp.einsum('hqk,khd->hqd', weights.astype(jnp.bfloat16), value_part, pref...  17.9 us
    dot_general x8, matrix products, per_device(): jnp.dot(scaled, weight, preferred_element_type=jnp.float32)  17.7 us
    reduce_sum x1, other arithmetic, attend(): totals = jnp.sum(weights, axis=2)  17.6 us
  transfers between devices with their start and end apart: 3, of which 2 were waited for; matrix products, arithmetic and copies ran while one was open for 14% of the time, Pallas kernels for 0%

commit v1 on v0

--- a/solution.py
+++ b/solution.py
@@ -9,6 +9,11 @@
 EPSILON = 1e-06
 ROTARY_BASE = 10000.0
 NEGATIVE = -1e30
+
+
+def gather_by_exchange(x, axis, dim):
+    copies = jnp.concatenate([x] * lax.axis_size(axis), axis=dim)
+    return lax.all_to_all(copies, axis, dim, dim, tiled=True)
 
 
 def carried_in(part, axis, combine, identity):
@@ -200,7 +205,7 @@
         input_gate_weight,
         forget_gate_weight,
     )
-    floats = lax.all_gather(inputs, "tp", axis=1, tiled=True).astype(jnp.float32)
+    floats = gather_by_exchange(inputs, "tp", 1).astype(jnp.float32)
     scaled = (floats * norm_gain[None, :]).astype(jnp.bfloat16)
     running_sums = tuple(
         (jnp.dot(scaled, weight, preferred_element_type=jnp.float32) for weight in weights)

time: 311 us -> 368 us (1.18)
  local copies, waits for them, and re-layouts: 22.1 us -> 43.5 us
  other arithmetic: 36.2 us -> 56.4 us
  waiting for transfers between devices: 60.4 us -> 70.7 us
  matrix products: 75.5 us -> 70.9 us
  starting transfers between devices: 0.12 us -> 4.42 us
    all_gather x1 -> x0, waiting for transfers between devices: 21.1 us -> none  [per_device(): lax.all_gather(inputs, 'tp', axis=1, tiled=True).astype(jnp.float32)]
    all_to_all x0 -> x1, waiting for transfers between devices: none -> 16.9 us  [gather_by_exchange(): return lax.all_to_all(copies, axis, dim, dim, tiled=True)]
    reduce_scatter x1, waiting for transfers between devices: 38.5 us -> 53.7 us  [per_device(): lax.psum_scatter(partial_term.astype(jnp.bfloat16), 'tp', scatter_dimensi...]
    dynamic_update_slice x18, local copies, waits for them, and re-layouts: 7.69 us -> 19.3 us  [memory_blocks(): lax.scan(scan_step, entering, entries)]
    add x6, other arithmetic: 0.47 us -> 8.04 us  [advance_state(): former[:, None] * normal + latter[:, None] * block_normal]
    dot_general x8, matrix products: 17.7 us -> 11.7 us  [per_device(): jnp.dot(scaled, weight, preferred_element_type=jnp.float32)]
    all_to_all x0 -> x1, starting transfers between devices: none -> 4.34 us  [gather_by_exchange(): return lax.all_to_all(copies, axis, dim, dim, tiled=True)]
    exp x6, other arithmetic: 0.06 us -> 4.14 us  [advance_state(): latter = jnp.exp(block_max - new_stable)]
  transfers between devices with their start and end apart: 3 -> 3, of which waited for: 2 -> 2; matrix products, arithmetic and copies ran while one was open for 14% -> 21% of each run, Pallas kernels for 0% -> 0%
where the time goes in v1:
time: 368 us; the launch traced here: 365 us
  blocking collectives  104 us (28%)
  matrix products  70.9 us (19%)
  waiting for transfers between devices  70.7 us (19%)
  other arithmetic  56.4 us (15%)
  local copies, waits for them, and re-layouts  43.5 us (12%)
  between operations  14.8 us (4%)
  starting transfers between devices  4.42 us (1%)
    all_gather x3, blocking collectives, carried_in(): gathered = jax.tree.map(lambda a: lax.all_gather(a, axis), part)  81.8 us
    reduce_scatter x1, waiting for transfers between devices, per_device(): lax.psum_scatter(partial_term.astype(jnp.bfloat16), 'tp', scatter_dimensi...  53.7 us
    dot_general x2, matrix products, attend(): jnp.einsum('qhd,khd->hqk', query_side, key_side, preferred_element_type=j...  27.9 us
    unnamed x1, blocking collectives  22.4 us
    dynamic_update_slice x18, local copies, waits for them, and re-layouts, memory_blocks(): lax.scan(scan_step, entering, entries)  19.3 us
    dot_general x2, matrix products, attend(): jnp.einsum('hqk,khd->hqd', weights.astype(jnp.bfloat16), value_part, pref...  17.9 us
    reduce_sum x1, other arithmetic, attend(): totals = jnp.sum(weights, axis=2)  17.6 us
    all_to_all x1, waiting for transfers between devices, gather_by_exchange(): return lax.all_to_all(copies, axis, dim, dim, tiled=True)  16.9 us
  transfers between devices with their start and end apart: 3, of which 2 were waited for; matrix products, arithmetic and copies ran while one was open for 21% of the time, Pallas kernels for 0%

profile of v1, /device:TPU:0, one launch (start us, length us, event | category | flops | bytes accessed | tf_op | source)
XLA Modules:
  0.0 365.0 jit_solution(14279131620874310758)
XLA Ops:
  9.6 4.3 %all-to-all-start = ((bf16[384,4,512]{2,0,1:T(8,128)(2,1)}), bf16[384,4,512]{2,0,1:T(8,128)(2,1)}, u32[]{:S(2)}, u32[]{:S(2)}) async-start(bf16[384,4,512]{2,0,1:T(8,128)(2,1)} %copy.77), calls=%async_computation | async-start | bytes 3145728 | tf_op jit(solution)/shard_map/all_to_all | solution.py:16
  17.9 16.9 %all-to-all-done = bf16[384,4,512]{2,0,1:T(8,128)(2,1)} async-done(((bf16[384,4,512]{2,0,1:T(8,128)(2,1)}), bf16[384,4,512]{2,0,1:T(8,128)(2,1)}, u32[]{:S(2)}, u32[]{:S(2)}) %all-to-all-start) | async-done | bytes 1572896 | tf_op jit(solution)/shard_map/all_to_all | solution.py:16
  34.8 1.9 copy.78
  38.3 1.7 fusion.25
  43.2 22.4 %all-reduce = f32[32]{0:T(128)S(1)} all-reduce(f32[32]{0:T(128)S(1)} %dynamic-update-slice), channel_id=2, replica_groups=mesh['sp'=8,'tp'=4] {'sp'}, use_global_device_ids=true, to_apply=%add | all-reduce | flops 32 | bytes 256
  66.3 16.9 %all-gather.3 = f32[8,1,4]{2,1,0:T(1,128)} all-gather(f32[1,1,4]{2,1,0:T(1,128)S(1)} %bitcast.236), channel_id=1, replica_groups=mesh['sp'=8,'tp'=4] {'sp'}, dimensions={0}, use_global_device_ids=true | all-gather | bytes 144 | tf_op jit(solution)/shard_map/all_gather | solution.py:21
  85.8 2.0 fusion.45
  89.7 2.1 fusion.43
  96.7 26.9 %all-gather.4 = f32[8,4,64]{2,1,0:T(4,128)} all-gather(f32[1,4,64]{2,1,0:T(4,128)S(1)} %bitcast.235), channel_id=4, replica_groups=mesh['sp'=8,'tp'=4] {'sp'}, dimensions={0}, use_global_device_ids=true | all-gather | bytes 9216 | tf_op jit(solution)/shard_map/all_gather | solution.py:21
  126.9 2.1 fusion.80
  130.6 2.4 fusion.77
  133.0 38.1 %all-gather.1 = f32[32,64,64]{2,1,0:T(8,128)} all-gather(f32[4,64,64]{2,1,0:T(8,128)S(1)} %copy-done.11), channel_id=3, replica_groups=mesh['sp'=8,'tp'=4] {'sp'}, dimensions={0}, use_global_device_ids=true | all-gather | bytes 589824 | tf_op jit(solution)/shard_map/all_gather | solution.py:21
  176.2 44.6 %while.37 = (s32[]{:T(128)}, f32[4,64,64]{2,1,0:T(8,128)S(1)}, f32[4,64]{1,0:T(4,128)}, f32[4]{0:T(128)}, f32[6,4,64,64]{3,2,0,1:T(8,128)}, /*index=5*/f32[6,4,6...) while((s32[]{:T(128)}, f32[4,64,64]{2,1,0:T(8,128)S(1)}, ...), condition=%wide.region_14.15_spmd, body=%wide.region_13.14_spmd.sunk | while | flops 49938 | bytes 400769 | solution.py:92
  220.9 2.7 fusion.49
  225.3 1.9 reshape.203
  227.2 1.9 copy.107
  235.6 2.0 fusion.42
  237.7 10.3 %fusion.74 = f32[4,384,3072]{2,1,0:T(8,128)} fusion(bf16[3072,4,128]{0,2,1:T(8,128)(2,1)} %all-gather.7.cloned.1.call-done, bf16[384,4,16]{0,2,1:T(8,128)(2,1)S(1)} %get-tuple-element.274, bf16[384,4,16]{0,2,1:T(8,128)(2,1)S(1)} %get-tuple-element.275), kind=kOutput, calls=%fused_computation.82 | convolution fusion | flops 302186496 | bytes 19759104 | tf_op jit(solution)/shard_map/qhd,khd->hqk/dot_general | solution.py:162
  248.1 17.5 %fusion.14 = (f32[4,384]{1,0:T(4,128)S(1)}, f32[4,384]{1,0:T(4,128)S(1)}, f32[4,384,3072]{2,1,0:T(8,128)}) fusion(pred[384,3072]{1,0:T(8,128)(4,1)S(1)} %copy-done.3, f32[4,384,3072]{2,1,0:T(8,128)} %fusion.74, bf16[3072,4,128]{0,2,1:T(8,128)(2,1)} %all-gather.7.cloned.1.call-done, bf16[384,4,16]{0,2,1:T(8,128)(2,1)S(1)} %get-tuple-element.267, ...), kind=kOutput, calls=%fused_computation.32 | convolution fusion | flops 330494976 | bytes 39825408 | tf_op jit(solution)/shard_map/qhd,khd->hqk/dot_general | solution.py:162
  265.6 17.6 %fusion.17 = (f32[4,384]{1,0:T(4,128)S(1)}, f32[4,384]{1,0:T(4,128)S(1)}) fusion(f32[4,384,3072]{2,1,0:T(8,128)} %get-tuple-element.278, f32[4,384]{1,0:T(4,128)S(1)} %get-tuple-element.285, pred[384,3072]{1,0:T(8,128)(4,1)} %iota_compare_fusion, f32[4,384]{1,0:T(4,128)S(1)} %get-tuple-element.286, f32[4,384,3072]{2,1,0:T(8,128)} %fusion.74), kind=kLoop, calls=%fused_computation.35 | loop fusion | flops 47182848 | bytes 38952960 | tf_op jit(solution)/shard_map/reduce_sum | solution.py:168
  283.5 8.0 %fusion.67 = f32[384,4,64]{0,2,1:T(8,128)S(1)} fusion(bf16[3072,4,128]{0,2,1:T(8,128)(2,1)} %all-gather.7.cloned.1.call-done, f32[4,384,3072]{2,1,0:T(8,128)S(1)} %copy-done.1, f32[4,384]{1,0:T(4,128)S(1)} %get-tuple-element.286, pred[384,3072]{1,0:T(8,128)(4,1)} %iota_compare_fusion, f32[384,4]{0,1:T(4,128)S(1)} %bitcast.239), kind=kOutput, calls=%fused_computation.79 | convolution fusion | flops 627671040 | bytes 22032384 | tf_op jit(solution)/shard_map/hqk,khd->hqd/dot_general | solution.py:169
  291.5 9.9 %multiply_reduce_fusion.1 = (f32[384,4]{0,1:T(4,128)S(1)}, f32[384,4,64]{0,2,1:T(8,128)S(1)}) fusion(f32[384,4,64]{0,2,1:T(8,128)S(1)} %fusion.67, f32[384,4]{0,1:T(4,128)S(1)} %bitcast.238, bf16[3072,4,128]{0,2,1:T(8,128)(2,1)} %all-gather.7.cloned.1.call-done, f32[4,384,3072]{2,1,0:T(8,128)} %get-tuple-element.278, f32[4,384]{1,0:T(4,128)S(1)} %get-tuple-element.285, ...), kind=kOutput, calls=%fused_computation.97 | convolution fusion | flops 628062720 | bytes 22431760 | tf_op jit(solution)/shard_map/hqk,khd->hqd/dot_general | solution.py:169
  302.6 1.8 add_convert_fusion
  304.4 53.7 %reduce-scatter.2.cloned.1.call-done = bf16[384,512]{1,0:T(8,128)(2,1)} async-done(((bf16[384,2048]{1,0:T(8,128)(2,1)}), bf16[384,512]{1,0:T(8,128)(2,1)}) %reduce-scatter.2.cloned.1.call-update) | async-done | bytes 393232 | tf_op jit(solution)/shard_map/reduce_scatter | solution.py:278
  (194 shorter events, 85.1 us)
Async XLA Ops:
  6.5 295.0 %copy-start = (bf16[256,2048]{1,0:T(8,128)(2,1)S(1)}, bf16[256,2048]{1,0:T(8,128)(2,1)}, u32[]{:S(2)}) copy-start(bf16[256,2048]{1,0:T(8,128)(2,1)} %param.34) | copy-start | bytes 3145732
  8.0 6.1 %copy-start.33 = (u32[32]{0:T(128)S(1)}, u32[32]{0:T(128)}, u32[]{:S(2)}) copy-start(u32[32]{0:T(128)} %constant.98) | copy-start | bytes 388
  9.6 25.2 %all-to-all-start = ((bf16[384,4,512]{2,0,1:T(8,128)(2,1)}), bf16[384,4,512]{2,0,1:T(8,128)(2,1)}, u32[]{:S(2)}, u32[]{:S(2)}) async-start(bf16[384,4,512]{2,0,1:T(8,128)(2,1)} %copy.77), calls=%async_computation | async-start | bytes 3145728 | tf_op jit(solution)/shard_map/all_to_all | solution.py:16
  14.0 24.3 %copy-start.24 = (f32[2048]{0:T(1024)S(1)}, f32[2048]{0:T(1024)}, u32[]{:S(2)}) copy-start(f32[2048]{0:T(1024)} %param.21) | copy-start | bytes 24580
  14.0 223.7 %all-gather.7.cloned.1.call-start = ((), (), s32[]{:S(2)}) async-start(), calls=%async_computation.2 | async-start | bytes 3538944 | tf_op jit(solution)/shard_map/all_gather | solution.py:238
  16.2 107.6 %copy-start.7 = (f32[384,16]{0,1:T(8,128)}, f32[384,16]{0,1:T(8,128)S(1)}, u32[]{:S(2)}) copy-start(f32[384,16]{0,1:T(8,128)S(1)} %get-tuple-element.276) | copy-start | bytes 73732
  16.2 107.6 %copy-start.9 = (f32[384,16]{0,1:T(8,128)}, f32[384,16]{0,1:T(8,128)S(1)}, u32[]{:S(2)}) copy-start(f32[384,16]{0,1:T(8,128)S(1)} %get-tuple-element.277) | copy-start | bytes 73732
  37.9 4.5 %copy-start.22 = (bf16[2048,4]{0,1:T(4,128)(2,1)S(1)}, bf16[2048,4]{0,1:T(4,128)(2,1)}, u32[]{:S(2)}) copy-start(bf16[2048,4]{0,1:T(4,128)(2,1)} %param.28) | copy-start | bytes 49156
  40.1 53.2 %copy-start.19 = (f32[384]{0:T(512)}, f32[384]{0:T(512)S(1)}, u32[]{:S(2)}) copy-start(f32[384]{0:T(512)S(1)} %add_rsqrt_fusion.1) | copy-start | bytes 4612
  42.9 48.9 %copy-start.14 = (f32[6,64,4]{1,0,2:T(8,128)}, f32[6,64,4]{1,0,2:T(8,128)S(1)}, u32[]{:S(2)}) copy-start(f32[6,64,4]{1,0,2:T(8,128)S(1)} %reshape.201) | copy-start | bytes 18436
  84.4 7.4 %copy-start.17 = (f32[4,6,64]{2,1,0:T(8,128)}, f32[4,6,64]{2,1,0:T(8,128)S(1)}, u32[]{:S(2)}) copy-start(f32[4,6,64]{2,1,0:T(8,128)S(1)} %subtract_exponential_fusion.4) | copy-start | bytes 18436
  124.8 8.2 %copy-start.11 = (f32[4,64,64]{2,1,0:T(8,128)S(1)}, f32[4,64,64]{2,1,0:T(8,128)}, u32[]{:S(2)}) copy-start(f32[4,64,64]{2,1,0:T(8,128)} %fusion.83) | copy-start | bytes 196612
  125.5 232.6 %reduce-scatter.2.cloned.1.call-start = ((), (), s32[]{:S(2)}) async-start(), calls=%async_computation.3 | async-start | bytes 1966080 | tf_op jit(solution)/shard_map/reduce_scatter | solution.py:278
  220.8 8.3 %copy-start.23 = (f32[6,4]{1,0:T(8,128)S(1)}, f32[6,4]{1,0:T(8,128)}, u32[]{:S(2)}) copy-start(f32[6,4]{1,0:T(8,128)} %get-tuple-element.124) | copy-start | bytes 292
  220.8 8.5 %copy-start.15 = (f32[6,64,4]{1,0,2:T(8,128)S(1)}, f32[6,64,4]{1,0,2:T(8,128)}, u32[]{:S(2)}) copy-start(f32[6,64,4]{1,0,2:T(8,128)} %copy-done.14) | copy-start | bytes 18436
  220.8 8.5 %copy-start.18 = (pred[64,64]{0,1:T(8,128)(4,1)S(1)}, pred[64,64]{0,1:T(8,128)(4,1)}, u32[]{:S(2)}) copy-start(pred[64,64]{0,1:T(8,128)(4,1)} %iota_compare_fusion.1) | copy-start | bytes 12292
  220.9 9.1 %copy-start.31 = (f32[6,4,64]{2,1,0:T(4,128)S(1)}, f32[6,4,64]{2,1,0:T(4,128)}, u32[]{:S(2)}) copy-start(f32[6,4,64]{2,1,0:T(4,128)} %get-tuple-element.126) | copy-start | bytes 18436
  229.3 3.9 %copy-start.5 = (bf16[6,64,4,64]{3,2,1,0:T(4,128)(2,1)S(1)}, bf16[6,64,4,64]{3,2,1,0:T(4,128)(2,1)}, u32[]{:S(2)}) copy-start(bf16[6,64,4,64]{3,2,1,0:T(4,128)(2,1)} %reshape.202) | copy-start | bytes 589828
  229.3 4.7 %copy-start.13 = (bf16[4,6,64,64]{2,3,1,0:T(8,128)(2,1)S(1)}, bf16[4,6,64,64]{2,3,1,0:T(8,128)(2,1)}, u32[]{:S(2)}) copy-start(bf16[4,6,64,64]{2,3,1,0:T(8,128)(2,1)} %copy.107) | copy-start | bytes 589828
  229.3 4.7 %copy-start.30 = (f32[6,4,64,64]{3,2,0,1:T(8,128)S(1)}, f32[6,4,64,64]{3,2,0,1:T(8,128)}, u32[]{:S(2)}) copy-start(f32[6,4,64,64]{3,2,0,1:T(8,128)} %get-tuple-element.125) | copy-start | bytes 1179652
  237.7 10.4 %copy-start.3 = (pred[384,3072]{1,0:T(8,128)(4,1)S(1)}, pred[384,3072]{1,0:T(8,128)(4,1)}, u32[]{:S(2)}) copy-start(pred[384,3072]{1,0:T(8,128)(4,1)} %iota_compare_fusion) | copy-start | bytes 3538948
  265.6 17.9 %copy-start.1 = (f32[4,384,3072]{2,1,0:T(8,128)S(1)}, f32[4,384,3072]{2,1,0:T(8,128)}, u32[]{:S(2)}) copy-start(f32[4,384,3072]{2,1,0:T(8,128)} %fusion.74) | copy-start | bytes 56623108
  283.5 8.0 %copy-start.32 = (f32[4]{0:T(128)S(1)}, f32[4]{0:T(128)}, u32[]{:S(2)}) copy-start(f32[4]{0:T(128)} %param.32) | copy-start | bytes 52
  291.5 9.9 %copy-start.27 = (f32[64]{0:T(128)S(1)}, f32[64]{0:T(128)}, u32[]{:S(2)}) copy-start(f32[64]{0:T(128)} %param.33) | copy-start | bytes 772
  (13 other events, 26.5 us)
Sparse Core Ops, SparseCore 0:
  125.7 67.2 all-gather.6
  304.6 53.5 reduce-scatter.1
